TPU v7x, 32 devices: a whole 2x2x4 slice. The times are simulated.
32 devices in a mesh: gr: 2 (over x), fs: 8 (over z, y), tp: 2 (over core).
Axes of the slice: x: 2, y: 2, z: 4, core: 2. Of those that a mesh axis runs over, the one named last changes fastest.
Arguments:
- prompt: bfloat16 [4, 256, 2048], P(('gr', 'tp')), as said below
- norm_gain: float32 [2, 2048], P(None, 'fs'), may hold values from 0.1 to 1.9
- gate_weight: float32 [2, 2048, 4096], P(None, 'fs', ('gr', 'tp')), may hold values from -0.125 to 0.125
- up_weight: float32 [2, 2048, 4096], P(None, 'fs', ('gr', 'tp')), may hold values from -0.125 to 0.125
- down_weight: float32 [2, 4096, 2048], P(None, 'fs', ('gr', 'tp')), may hold values from -0.09375 to 0.09375
Outputs:
- gate_sampler: bfloat16 [2, 2048, 4096], P(None, None, 'fs')
- up_sampler: bfloat16 [2, 2048, 4096], P(None, None, 'fs')
- down_sampler: bfloat16 [2, 4096, 2048], P(None, 'fs')
- mixed: bfloat16 [4, 256, 2048], P(('gr', 'tp'))
Inputs may be any that keep to these rules, and one draw needn't show every extreme that they name: prompt features have scales that differ from feature to feature.
All inputs are finite; a program needn't handle non-finite values.
Results may differ from a plain program's by a relative error of at most 0.0043.
Values may be sent and summed in bfloat16 or wider, within the bound.
A program may use at most 64 MiB of HBM per device.

v0:
```python
import functools

import jax
import jax.numpy as jnp
from jax import lax
from jax.experimental import pallas as pl
from jax.experimental.pallas import tpu as pltpu
from jax.sharding import PartitionSpec as P

norm_eps = 1e-06
MESH = pl.DeviceIdType.MESH
f32 = jnp.float32
bf16 = jnp.bfloat16


def kernel(G, n, T, prompt, gain, gate_w, up_w, down_w,
           wall, dn, ag,
           wsrc, p, r1, q2, r2, lhs, hid, st,
           x_s, x_r, v_s, v_r, xd_s, p_s, w_r, w_l, f_s, d_s, d_r,
           s1_s, s1_r, s2_s, s2_r, g_s, g_r, h_s):
    gr, fs, tp = lax.axis_index("gr"), lax.axis_index("fs"), lax.axis_index("tp")
    q, R, FFb = wsrc.shape[3:]
    tb, D = prompt.shape[1:]
    rows = n * tb
    DC = dn.shape[3]
    na = n // 2
    a, b = fs // 2, lax.rem(fs, 2)
    peer = fs + 1 - 2 * b
    is_recv = lax.rem(fs // q, T) == tp
    slot_me = gr * T + tp
    h = (R * 4 // 16) // 16 * 16 if G == 2 else 0
    m = R - h

    def mine(g):
        return pl.ds(pl.multiple_of(g * h, 16), m) if h else pl.ds(0, R)

    def only(g):
        return pl.ds(pl.multiple_of(g * m, 16), h)

    def dev(g, f, t):
        return {"gr": g, "fs": f, "tp": t}

    def rc(src, dst, ss, rs, d):
        return pltpu.make_async_remote_copy(
            src_ref=src, dst_ref=dst, send_sem=ss, recv_sem=rs,
            device_id=d, device_id_type=MESH)

    def loop(lo, hi, body):
        def step(i, c):
            body(i)
            return c
        lax.fori_loop(lo, hi, step, 0)

    others_g = [lax.rem(gr + d, G) for d in range(1, G)]
    others_t = [lax.rem(tp + d, T) for d in range(1, T)]

    def x_copy(k, w, i, g_src, g_dst):
        blk = wsrc.at[k, w, g_src, i, mine(g_dst)]
        return rc(blk, blk, x_s.at[k, w, i, g_dst], x_r.at[k, w, i, g_src], dev(g_dst, fs, tp))

    def xd_copy(k, g_src, g_dst):
        blk = dn.at[k, g_src * T + tp]
        return rc(blk, blk, xd_s.at[k, g_dst], d_r.at[k, g_src * T + tp], dev(g_dst, fs, tp))

    def d_copy(k, g_src, t_src, t_dst):
        blk = dn.at[k, g_src * T + t_src]
        return rc(blk, blk, d_s.at[k, g_src, t_dst], d_r.at[k, g_src * T + t_src], dev(gr, fs, t_dst))

    def col_of(g, i):
        return (g * T + tp) * q + i

    def p_copy(k, w, g, i):
        return rc(wsrc.at[k, w, g, i, mine(gr)], wall.at[k, w, fs, mine(gr)], p_s.at[k, w, g, i],
                  w_r.at[k, w, fs], dev(gr, col_of(g, i), tp))

    def l_copy(k, w, g, i):
        return pltpu.make_async_copy(wsrc.at[k, w, g, i, mine(gr)], wall.at[k, w, fs, mine(gr)], w_l.at[k, w])

    def f_copy(k, w, f, t):
        blk = wall.at[k, w, f, mine(gr)]
        return rc(blk, blk, f_s.at[k, w, 0, f, t], w_r.at[k, w, f], dev(gr, fs, t))

    def v_copy(k, w, f, g_src):
        blk = wall.at[k, w, f, only(g_src)]
        return rc(blk, blk, v_s.at[k, w, f], v_r.at[k, w, 0, f], dev(1 - g_src, fs, tp))

    def fv_copy(k, w, f, t):
        blk = wall.at[k, w, f, only(1 - gr)]
        return rc(blk, blk, f_s.at[k, w, 1, f, t], v_r.at[k, w, 1, f], dev(gr, fs, t))

    def cast_w(k, w):
        ref = (gate_w, up_w)[w]
        for i in range(q):
            wsrc[k, w, gr, i] = (gain[k] * ref[k, :, i * FFb:(i + 1) * FFb]).astype(bf16)

    def xsend_w(k, w):
        for i in range(q):
            for g in others_g:
                x_copy(k, w, i, gr, g).start()

    def cast_d(k):
        dn[k, slot_me] = down_w[k].astype(bf16)

    def xsend_d(k):
        for g in others_g:
            xd_copy(k, gr, g).start()
        for t in others_t:
            d_copy(k, gr, tp, t).start()

    def plane(k, w, g, i):
        c = col_of(g, i)

        @pl.when(c != fs)
        def _():
            p_copy(k, w, g, i).start()

        @pl.when(c == fs)
        def _():
            l_copy(k, w, g, i).start()

    def plane_own(k, w):
        for i in range(q):
            plane(k, w, gr, i)

    def plane_x(k, w):
        for g in others_g:
            for i in range(q):
                x_copy(k, w, i, g, gr).wait_recv()
                plane(k, w, g, i)

    def gather_w(k, w):
        def forward(f):
            for t in others_t:
                f_copy(k, w, f, t).start()
            if h:
                v_copy(k, w, f, gr).start()

        @pl.when(is_recv)
        def _():
            l_copy(k, w, 0, 0).wait()
            forward(fs)

            def arrive(s):
                f = lax.rem(fs + s, n)
                f_copy(k, w, f, tp).wait_recv()
                forward(f)
            loop(1, n, arrive)

            if h:
                def cross(s):
                    f = lax.rem(fs + s, n)
                    v_copy(k, w, f, 1 - gr).wait_recv()
                    for t in others_t:
                        fv_copy(k, w, f, t).start()
                loop(0, n, cross)

        @pl.when(jnp.logical_not(is_recv))
        def _():
            def arrive(f):
                f_copy(k, w, f, tp).wait_recv()
                if h:
                    fv_copy(k, w, f, tp).wait_recv()
            loop(0, n, arrive)

    def gather_d(k):
        for g in others_g:
            xd_copy(k, g, gr).wait_recv()
            for t in others_t:
                d_copy(k, g, tp, t).start()
        for g in range(G):
            for t in others_t:
                d_copy(k, g, t, tp).wait_recv()

    def gather_done(k):
        for w in range(2):
            for i in range(q):
                for g in others_g:
                    x_copy(k, w, i, gr, g).wait_send()
            for g in range(G):
                for i in range(q):
                    @pl.when(col_of(g, i) != fs)
                    def _():
                        p_copy(k, w, g, i).wait_send()

            @pl.when(is_recv)
            def _():
                def sent(f):
                    for t in others_t:
                        f_copy(k, w, f, t).wait_send()
                        if h:
                            fv_copy(k, w, f, t).wait_send()
                    if h:
                        v_copy(k, w, f, gr).wait_send()
                loop(0, n, sent)
        for g in others_g:
            xd_copy(k, gr, g).wait_send()
        for g in range(G):
            for t in others_t:
                d_copy(k, g, tp, t).wait_send()

    def flatten(ref):
        cw = 256

        def chunk(j):
            cols = pl.ds(pl.multiple_of(j * cw, cw), cw)
            lhs[:, cols] = ref[:, :, cols].astype(f32).reshape(rows, cw).astype(bf16)
        loop(0, D // cw, chunk)

    def normed_of(x):
        return (x * lax.rsqrt(jnp.mean(x * x, axis=-1, keepdims=True) + norm_eps)).astype(bf16)

    def compute(k):
        ft = min(FFb, 256)

        def act(j):
            cols = pl.ds(pl.multiple_of(j * ft, ft), ft)
            gate = jnp.dot(lhs[...], wall[k, 0, :, :, cols].reshape(D, ft), preferred_element_type=f32)
            up = jnp.dot(lhs[...], wall[k, 1, :, :, cols].reshape(D, ft), preferred_element_type=f32)
            hid[:, cols] = (gate / (1.0 + jnp.exp(-gate)) * up).astype(bf16)
        loop(0, FFb // ft, act)

        def proj(s):
            cols = pl.ds(pl.multiple_of(s * DC, DC), DC)
            v = jnp.dot(hid[...], dn[k, s], preferred_element_type=f32)
            p[k, :, :, cols] = v.reshape(n, tb, DC).astype(bf16)
        loop(0, G * T, proj)

    def s1_copy(k, a2):
        return rc(p.at[k, 2 * a2 + 1 - b], r1.at[k, a2], s1_s.at[k, a2], s1_r.at[k, a2], dev(gr, peer, tp))

    def s2_copy(k, a2, a_from):
        return rc(q2.at[k, a2], r2.at[k, a_from], s2_s.at[k, a2], s2_r.at[k, a_from],
                  dev(gr, 2 * a2 + b, tp))

    def rs_first(k):
        def send(d):
            s1_copy(k, lax.rem(a + d, na)).start()
        loop(1, na + 1, send)

    def rs_second(k):
        def send(d):
            a2 = lax.rem(a + d, na)
            s1_copy(k, a2).wait_recv()
            q2[k, a2] = (p[k, 2 * a2 + b].astype(f32) + r1[k, a2].astype(f32)).astype(bf16)
            s2_copy(k, a2, a).start()
        loop(1, na, send)
        s1_copy(k, a).wait_recv()
        st[...] += 0.5 * (p[k, fs].astype(f32) + r1[k, a].astype(f32))

    def rs_last(k):
        def take(d):
            a2 = lax.rem(a + d, na)
            s2_copy(k, a2, a2).wait_recv()
            st[...] += 0.5 * r2[k, a2].astype(f32)
        loop(1, na, take)

    def rs_done(k):
        def sent(a2):
            s1_copy(k, a2).wait_send()
        loop(0, na, sent)

        def sent2(d):
            s2_copy(k, lax.rem(a + d, na), a).wait_send()
        loop(1, na, sent2)

    def z_copy(k, j, a2):
        return rc(ag.at[k, j], ag.at[k, j], g_s.at[k, a2], g_r.at[k, j], dev(gr, 2 * a2 + b, tp))

    def y_copy(k, j):
        return rc(ag.at[k, j], ag.at[k, j], h_s.at[k, j // 2], g_r.at[k, j], dev(gr, peer, tp))

    def ag_start(k):
        def send(d):
            z_copy(k, fs, lax.rem(a + d, na)).start()
        loop(1, na, send)
        y_copy(k, fs).start()

    def ag_rest(k):
        def relay(d):
            a2 = lax.rem(a + d, na)
            z_copy(k, 2 * a2 + b, a2).wait_recv()
            y_copy(k, 2 * a2 + b).start()
        loop(1, na, relay)

        def take(a2):
            y_copy(k, 2 * a2 + 1 - b).wait_recv()
        loop(0, na, take)

    def ag_done(k):
        def sent(d):
            z_copy(k, fs, lax.rem(a + d, na)).wait_send()
        loop(1, na, sent)

        def sent2(a2):
            y_copy(k, 2 * a2 + b).wait_send()
        loop(0, na, sent2)

    barrier = pltpu.get_barrier_semaphore()

    def greet(s):
        pl.semaphore_signal(barrier, inc=1, device_id=dev(gr, lax.rem(fs + s, n), tp), device_id_type=MESH)
    loop(1, n, greet)
    for t in others_t:
        pl.semaphore_signal(barrier, inc=1, device_id=dev(gr, fs, t), device_id_type=MESH)
    for g in others_g:
        pl.semaphore_signal(barrier, inc=1, device_id=dev(g, fs, tp), device_id_type=MESH)
    cast_w(0, 0)
    pl.semaphore_wait(barrier, n + T + G - 3)

    xsend_w(0, 0)
    plane_own(0, 0)
    cast_w(0, 1)
    xsend_w(0, 1)
    plane_own(0, 1)
    cast_d(0)
    xsend_d(0)
    cast_w(1, 0)
    cast_w(1, 1)
    cast_d(1)

    def norm_rows(j):
        p[0, j] = normed_of(prompt[j].astype(f32))
    loop(0, n, norm_rows)
    flatten(p.at[0])
    st[...] = prompt[fs].astype(f32)

    plane_x(0, 0)
    plane_x(0, 1)
    xsend_w(1, 0)
    plane_own(1, 0)
    xsend_w(1, 1)
    plane_x(1, 0)
    plane_own(1, 1)
    plane_x(1, 1)
    gather_w(0, 0)
    gather_w(0, 1)
    xsend_d(1)
    gather_d(0)
    compute(0)
    rs_first(0)
    rs_second(0)
    rs_last(0)
    ag[0, fs] = normed_of(st[...])
    ag_start(0)
    gather_w(1, 0)
    ag_rest(0)
    flatten(ag.at[0])
    gather_w(1, 1)
    gather_d(1)
    compute(1)
    rs_first(1)
    rs_second(1)
    rs_last(1)
    ag[1, fs] = st[...].astype(bf16)
    ag_start(1)
    ag_rest(1)
    for k in range(2):
        gather_done(k)
        rs_done(k)
        ag_done(k)


def write_out(wall, dn, ag, gate_o, up_o, down_o, mixed_o, o_s, d_s, m_s):
    L, S, _, DC = dn.shape
    copies = []
    for k in range(L):
        copies.append(pltpu.make_async_copy(wall.at[k, 0], gate_o.at[k], o_s.at[k, 0]))
        copies.append(pltpu.make_async_copy(wall.at[k, 1], up_o.at[k], o_s.at[k, 1]))
        for s in range(S):
            copies.append(pltpu.make_async_copy(
                dn.at[k, s], down_o.at[k, :, pl.ds(s * DC, DC)], d_s.at[k, s]))
    copies.append(pltpu.make_async_copy(ag.at[L - 1], mixed_o, m_s))
    for c in copies:
        c.start()
    for c in copies:
        c.wait()


def per_device(G, n, T, prompt, norm_gain, gate_weight, up_weight, down_weight):
    D = prompt.shape[2]
    rows = prompt.shape[0] * prompt.shape[1]
    L, R, C = gate_weight.shape
    FFb, DC = down_weight.shape[1:]
    q = C // FFb
    tb = rows // n
    na = n // 2
    dma = pltpu.SemaphoreType.DMA
    vmem = pl.BlockSpec(memory_space=pltpu.VMEM)
    anym = pl.BlockSpec(memory_space=pl.ANY)
    wall, dn, ag = pl.pallas_call(
        functools.partial(kernel, G, n, T),
        out_shape=(
            pltpu.VMEM((L, 2, n, R, FFb), bf16),
            pltpu.VMEM((L, G * T, FFb, DC), bf16),
            pltpu.VMEM((L, n, tb, D), bf16),
        ),
        in_specs=[vmem] * 5,
        out_specs=(vmem,) * 3,
        scratch_shapes=[
            pltpu.VMEM((L, 2, G, q, R, FFb), bf16),
            pltpu.VMEM((L, n, tb, D), bf16),
            pltpu.VMEM((L, na, tb, D), bf16),
            pltpu.VMEM((L, na, tb, D), bf16),
            pltpu.VMEM((L, na, tb, D), bf16),
            pltpu.VMEM((rows, D), bf16),
            pltpu.VMEM((rows, FFb), bf16),
            pltpu.VMEM((tb, D), f32),
            dma((L, 2, q, G)), dma((L, 2, q, G)), dma((L, 2, n)), dma((L, 2, 2, n)), dma((L, G)),
            dma((L, 2, G, q)), dma((L, 2, n)), dma((L, 2)), dma((L, 2, 2, n, T)),
            dma((L, G, T)), dma((L, G * T)),
            dma((L, na)), dma((L, na)), dma((L, na)), dma((L, na)),
            dma((L, na)), dma((L, n)), dma((L, na)),
        ],
        compiler_params=pltpu.CompilerParams(
            collective_id=0, has_side_effects=True, vmem_limit_bytes=40 * 1024 * 1024),
    )(prompt.reshape(n, tb, D), norm_gain[:, :, None], gate_weight, up_weight, down_weight)
    gate, up, down, mixed = pl.pallas_call(
        write_out,
        out_shape=(
            jax.ShapeDtypeStruct((L, n, R, FFb), bf16),
            jax.ShapeDtypeStruct((L, n, R, FFb), bf16),
            jax.ShapeDtypeStruct((L, FFb, D), bf16),
            jax.ShapeDtypeStruct((n, tb, D), bf16),
        ),
        in_specs=[anym] * 3,
        out_specs=(anym,) * 4,
        scratch_shapes=[dma((L, 2)), dma((L, G * T)), dma(())],
        compiler_params=pltpu.CompilerParams(vmem_limit_bytes=1024 * 1024),
    )(*(pltpu.with_memory_space_constraint(x, pltpu.VMEM) for x in (wall, dn, ag)))
    return (gate.reshape(L, n * R, FFb), up.reshape(L, n * R, FFb), down, mixed.reshape(prompt.shape))


def solution(mesh):
    G, n, T = mesh.shape["gr"], mesh.shape["fs"], mesh.shape["tp"]
    in_specs = (
        P(("gr", "tp"), None, None),
        P(None, "fs"),
        P(None, "fs", ("gr", "tp")),
        P(None, "fs", ("gr", "tp")),
        P(None, "fs", ("gr", "tp")),
    )
    out_specs = (
        P(None, None, "fs"),
        P(None, None, "fs"),
        P(None, "fs", None),
        P(("gr", "tp"), None, None),
    )
    return jax.shard_map(
        functools.partial(per_device, G, n, T),
        mesh=mesh, in_specs=in_specs, out_specs=out_specs, check_vma=False)
```

profile of v0, /device:TPU:0, one launch (start us, length us, event | category | flops | bytes accessed | tf_op | source)
XLA Modules:
  0.0 177.2 jit_solution(12312751287711603318)
XLA Ops:
  0.6 1.5 copy.9.gain
  2.2 170.0 %shard_map.84 = (bf16[2,2,8,256,512]{4,3,2,1,0:T(8,128)(2,1)S(1)}, bf16[2,4,512,512]{3,2,1,0:T(8,128)(2,1)S(1)}, bf16[2,8,32,2048]{3,2,1,0:T(8,128)(2,1)S(1)}) custom-call(bf16[8,32,2048]{2,1,0:T(8,128)(2,1)} %bitcast.5, f32[2,256,1]{2,1,0:T(8,128)} %copy.9.gain, f32[2,256,1024]{2,1,0:T(8,128)} %gate_w.1, f32[2,256,1024]{2,1,0:T(8,128)} %up_w.1, ...), custom_call_target="tpu_custom_call" | custom-call | tf_op jit(solution)/shard_map/pallas_call | solution.py:390
  172.2 5.0 %shard_map.85 = (bf16[2,8,256,512]{3,2,1,0:T(8,128)(2,1)}, bf16[2,8,256,512]{3,2,1,0:T(8,128)(2,1)}, bf16[2,512,2048]{2,1,0:T(8,128)(2,1)}, bf16[8,32,2048]{2,1,0:T(8,128)(2,1)}) custom-call(bf16[2,2,8,256,512]{4,3,2,1,0:T(8,128)(2,1)S(1)} %get-tuple-element.11.wall, bf16[2,4,512,512]{3,2,1,0:T(8,128)(2,1)S(1)} %get-tuple-element.12.dn, ...), custom_call_target="tpu_custom_call" | custom-call | tf_op jit(solution)/shard_map/pallas_call | solution.py:417
where the time goes:
time: 178 us; the launch traced here: 177 us
  Pallas kernels  175 us (98%)
    pallas_call x1, Pallas kernels, per_device(): pl.pallas_call(functools.partial(kernel, G, n, T), out_shape=(pltpu.VMEM(...  170 us
    pallas_call x1, Pallas kernels, per_device(): pl.pallas_call(write_out, out_shape=(jax.ShapeDtypeStruct((L, n, R, FFb),...  4.99 us

commit v1 on v0

--- a/solution.py
+++ b/solution.py
@@ -17,7 +17,7 @@
            wall, dn, ag,
            wsrc, p, r1, q2, r2, lhs, hid, st,
            x_s, x_r, v_s, v_r, xd_s, p_s, w_r, w_l, f_s, d_s, d_r,
-           s1_s, s1_r, s2_s, s2_r, g_s, g_r, h_s):
+           s1_s, s1_r, s2_s, s2_r, g_s, gg_s, g_r, h_s):
     gr, fs, tp = lax.axis_index("gr"), lax.axis_index("fs"), lax.axis_index("tp")
     q, R, FFb = wsrc.shape[3:]
     tb, D = prompt.shape[1:]
@@ -25,17 +25,18 @@
     DC = dn.shape[3]
     na = n // 2
     a, b = fs // 2, lax.rem(fs, 2)
+    C = s1_s.shape[2]
+    tc = tb // C
     peer = fs + 1 - 2 * b
     is_recv = lax.rem(fs // q, T) == tp
     slot_me = gr * T + tp
-    h = (R * 4 // 16) // 16 * 16 if G == 2 else 0
-    m = R - h
-
-    def mine(g):
-        return pl.ds(pl.multiple_of(g * h, 16), m) if h else pl.ds(0, R)
-
-    def only(g):
-        return pl.ds(pl.multiple_of(g * m, 16), h)
+    hs = [(R * c // 16) // 16 * 16 if G == 2 else 0 for c in (4, 8)]
+
+    def mine(k, g):
+        return pl.ds(pl.multiple_of(g * hs[k], 16), R - hs[k]) if hs[k] else pl.ds(0, R)
+
+    def only(k, g):
+        return pl.ds(pl.multiple_of(g * (R - hs[k]), 16), hs[k])
 
     def dev(g, f, t):
         return {"gr": g, "fs": f, "tp": t}
@@ -55,7 +56,7 @@
     others_t = [lax.rem(tp + d, T) for d in range(1, T)]
 
     def x_copy(k, w, i, g_src, g_dst):
-        blk = wsrc.at[k, w, g_src, i, mine(g_dst)]
+        blk = wsrc.at[k, w, g_src, i, mine(k, g_dst)]
         return rc(blk, blk, x_s.at[k, w, i, g_dst], x_r.at[k, w, i, g_src], dev(g_dst, fs, tp))
 
     def xd_copy(k, g_src, g_dst):
@@ -70,22 +71,22 @@
         return (g * T + tp) * q + i
 
     def p_copy(k, w, g, i):
-        return rc(wsrc.at[k, w, g, i, mine(gr)], wall.at[k, w, fs, mine(gr)], p_s.at[k, w, g, i],
+        return rc(wsrc.at[k, w, g, i, mine(k, gr)], wall.at[k, w, fs, mine(k, gr)], p_s.at[k, w, g, i],
                   w_r.at[k, w, fs], dev(gr, col_of(g, i), tp))
 
     def l_copy(k, w, g, i):
-        return pltpu.make_async_copy(wsrc.at[k, w, g, i, mine(gr)], wall.at[k, w, fs, mine(gr)], w_l.at[k, w])
+        return pltpu.make_async_copy(wsrc.at[k, w, g, i, mine(k, gr)], wall.at[k, w, fs, mine(k, gr)], w_l.at[k, w])
 
     def f_copy(k, w, f, t):
-        blk = wall.at[k, w, f, mine(gr)]
+        blk = wall.at[k, w, f, mine(k, gr)]
         return rc(blk, blk, f_s.at[k, w, 0, f, t], w_r.at[k, w, f], dev(gr, fs, t))
 
     def v_copy(k, w, f, g_src):
-        blk = wall.at[k, w, f, only(g_src)]
+        blk = wall.at[k, w, f, only(k, g_src)]
         return rc(blk, blk, v_s.at[k, w, f], v_r.at[k, w, 0, f], dev(1 - g_src, fs, tp))
 
     def fv_copy(k, w, f, t):
-        blk = wall.at[k, w, f, only(1 - gr)]
+        blk = wall.at[k, w, f, only(k, 1 - gr)]
         return rc(blk, blk, f_s.at[k, w, 1, f, t], v_r.at[k, w, 1, f], dev(gr, fs, t))
 
     def cast_w(k, w):
@@ -128,11 +129,11 @@
                 x_copy(k, w, i, g, gr).wait_recv()
                 plane(k, w, g, i)
 
-    def gather_w(k, w):
+    def arrive(k, w):
         def forward(f):
             for t in others_t:
                 f_copy(k, w, f, t).start()
-            if h:
+            if hs[k]:
                 v_copy(k, w, f, gr).start()
 
         @pl.when(is_recv)
@@ -140,33 +141,39 @@
             l_copy(k, w, 0, 0).wait()
             forward(fs)
 
-            def arrive(s):
+            def take(s):
                 f = lax.rem(fs + s, n)
                 f_copy(k, w, f, tp).wait_recv()
                 forward(f)
-            loop(1, n, arrive)
-
-            if h:
-                def cross(s):
+            loop(1, n, take)
+
+    def cross(k, w):
+        if hs[k]:
+            @pl.when(is_recv)
+            def _():
+                def take(s):
                     f = lax.rem(fs + s, n)
                     v_copy(k, w, f, 1 - gr).wait_recv()
                     for t in others_t:
                         fv_copy(k, w, f, t).start()
-                loop(0, n, cross)
-
+                loop(0, n, take)
+
+    def landed(k, w):
         @pl.when(jnp.logical_not(is_recv))
         def _():
-            def arrive(f):
+            def take(f):
                 f_copy(k, w, f, tp).wait_recv()
-                if h:
+                if hs[k]:
                     fv_copy(k, w, f, tp).wait_recv()
-            loop(0, n, arrive)
-
-    def gather_d(k):
+            loop(0, n, take)
+
+    def relay_d(k):
         for g in others_g:
             xd_copy(k, g, gr).wait_recv()
             for t in others_t:
                 d_copy(k, g, tp, t).start()
+
+    def landed_d(k):
         for g in range(G):
             for t in others_t:
                 d_copy(k, g, t, tp).wait_recv()
@@ -187,9 +194,9 @@
                 def sent(f):
                     for t in others_t:
                         f_copy(k, w, f, t).wait_send()
-                        if h:
+                        if hs[k]:
                             fv_copy(k, w, f, t).wait_send()
-                    if h:
+                    if hs[k]:
                         v_copy(k, w, f, gr).wait_send()
                 loop(0, n, sent)
         for g in others_g:
@@ -225,75 +232,126 @@
             p[k, :, :, cols] = v.reshape(n, tb, DC).astype(bf16)
         loop(0, G * T, proj)
 
-    def s1_copy(k, a2):
-        return rc(p.at[k, 2 * a2 + 1 - b], r1.at[k, a2], s1_s.at[k, a2], s1_r.at[k, a2], dev(gr, peer, tp))
-
-    def s2_copy(k, a2, a_from):
-        return rc(q2.at[k, a2], r2.at[k, a_from], s2_s.at[k, a2], s2_r.at[k, a_from],
-                  dev(gr, 2 * a2 + b, tp))
+    half = na // 2 if na % 2 == 0 else na
+    far = na // half - 1
+    pos = lax.rem(a, half)
+    mirror = lax.rem(a + half, na)
+
+    def near(d):
+        return a - pos + lax.rem(pos + d, half)
+
+    def partner(d):
+        e = lax.div(d, half) if far else 1
+        return lax.rem(a // half + 1 - e, far + 1) * half + lax.rem(pos + d + (e if far else 1), half)
+
+    def part(c):
+        return pl.ds(c * tc, tc)
+
+    def s1_copy(k, a2, c):
+        return rc(p.at[k, 2 * a2 + 1 - b, part(c)], r1.at[k, a2, part(c)],
+                  s1_s.at[k, a2, c], s1_r.at[k, a2, c], dev(gr, peer, tp))
+
+    def s2_copy(k, a2, a_from, c):
+        return rc(q2.at[k, a2, part(c)], r2.at[k, a_from, part(c)],
+                  s2_s.at[k, a2, c], s2_r.at[k, a_from, c], dev(gr, 2 * a2 + b, tp))
 
     def rs_first(k):
+        for c in range(C):
+            def send(d):
+                s1_copy(k, partner(d), c).start()
+            loop(0, na - 1, send)
+            s1_copy(k, a, c).start()
+
+    def rs_remote(k, c):
         def send(d):
-            s1_copy(k, lax.rem(a + d, na)).start()
-        loop(1, na + 1, send)
-
-    def rs_second(k):
+            a2 = partner(d)
+            s1_copy(k, a2, c).wait_recv()
+            q2[k, a2, part(c)] = (p[k, 2 * a2 + b, part(c)].astype(f32) + r1[k, a2, part(c)].astype(f32)).astype(bf16)
+            s2_copy(k, a2, a, c).start()
+        loop(0, na - 1, send)
+
+    def rs_own(k, c):
+        s1_copy(k, a, c).wait_recv()
+        st[part(c)] += 0.5 * (p[k, fs, part(c)].astype(f32) + r1[k, a, part(c)].astype(f32))
+
+    def rs_last(k, c):
+        def take(d):
+            a2 = partner(na - 2 - d)
+            s2_copy(k, a2, a2, c).wait_recv()
+            st[part(c)] += 0.5 * r2[k, a2, part(c)].astype(f32)
+        loop(0, na - 1, take)
+        x = st[part(c)]
+        ag[k, fs, part(c)] = normed_of(x) if k == 0 else x.astype(bf16)
+
+        if far:
+            z_copy(k, fs, mirror, c).start()
+
         def send(d):
-            a2 = lax.rem(a + d, na)
-            s1_copy(k, a2).wait_recv()
-            q2[k, a2] = (p[k, 2 * a2 + b].astype(f32) + r1[k, a2].astype(f32)).astype(bf16)
-            s2_copy(k, a2, a).start()
-        loop(1, na, send)
-        s1_copy(k, a).wait_recv()
-        st[...] += 0.5 * (p[k, fs].astype(f32) + r1[k, a].astype(f32))
-
-    def rs_last(k):
-        def take(d):
-            a2 = lax.rem(a + d, na)
-            s2_copy(k, a2, a2).wait_recv()
-            st[...] += 0.5 * r2[k, a2].astype(f32)
-        loop(1, na, take)
+            z_copy(k, fs, near(d), c).start()
+        loop(1, half, send)
+        y_copy(k, fs, c).start()
+
+    def z_copy(k, j, a2, c):
+        blk = ag.at[k, j, part(c)]
+        return rc(blk, blk, g_s.at[k, a2, c], g_r.at[k, j, c], dev(gr, 2 * a2 + b, tp))
+
+    def y_copy(k, j, c):
+        blk = ag.at[k, j, part(c)]
+        return rc(blk, blk, h_s.at[k, j // 2, c], g_r.at[k, j, c], dev(gr, peer, tp))
+
+    def zz_copy(k, a2, c):
+        blk = ag.at[k, 2 * mirror + b, part(c)]
+        return rc(blk, blk, gg_s.at[k, a2, c], g_r.at[k, 2 * mirror + b, c], dev(gr, 2 * a2 + b, tp))
+
+    def ag_relay(k, c):
+        def pass_on(a2):
+            z_copy(k, 2 * a2 + b, a2, c).wait_recv()
+            y_copy(k, 2 * a2 + b, c).start()
+
+        def own(d):
+            pass_on(near(d))
+        loop(1, half, own)
+        if far:
+            z_copy(k, 2 * mirror + b, a, c).wait_recv()
+
+            def spread(d):
+                zz_copy(k, near(d), c).start()
+            loop(1, half, spread)
+            y_copy(k, 2 * mirror + b, c).start()
+
+            def theirs(d):
+                pass_on(lax.rem(near(d) + half, na))
+            loop(1, half, theirs)
+
+    def ag_take(k):
+        for c in range(C):
+            def take(a2):
+                y_copy(k, 2 * a2 + 1 - b, c).wait_recv()
+            loop(0, na, take)
 
     def rs_done(k):
-        def sent(a2):
-            s1_copy(k, a2).wait_send()
-        loop(0, na, sent)
-
-        def sent2(d):
-            s2_copy(k, lax.rem(a + d, na), a).wait_send()
-        loop(1, na, sent2)
-
-    def z_copy(k, j, a2):
-        return rc(ag.at[k, j], ag.at[k, j], g_s.at[k, a2], g_r.at[k, j], dev(gr, 2 * a2 + b, tp))
-
-    def y_copy(k, j):
-        return rc(ag.at[k, j], ag.at[k, j], h_s.at[k, j // 2], g_r.at[k, j], dev(gr, peer, tp))
-
-    def ag_start(k):
-        def send(d):
-            z_copy(k, fs, lax.rem(a + d, na)).start()
-        loop(1, na, send)
-        y_copy(k, fs).start()
-
-    def ag_rest(k):
-        def relay(d):
-            a2 = lax.rem(a + d, na)
-            z_copy(k, 2 * a2 + b, a2).wait_recv()
-            y_copy(k, 2 * a2 + b).start()
-        loop(1, na, relay)
-
-        def take(a2):
-            y_copy(k, 2 * a2 + 1 - b).wait_recv()
-        loop(0, na, take)
+        for c in range(C):
+            def sent(a2):
+                s1_copy(k, a2, c).wait_send()
+            loop(0, na, sent)
+
+            def sent2(d):
+                s2_copy(k, partner(d), a, c).wait_send()
+            loop(0, na - 1, sent2)
 
     def ag_done(k):
-        def sent(d):
-            z_copy(k, fs, lax.rem(a + d, na)).wait_send()
-        loop(1, na, sent)
-
-        def sent2(a2):
-            y_copy(k, 2 * a2 + b).wait_send()
-        loop(0, na, sent2)
+        for c in range(C):
+            def sent(d):
+                z_copy(k, fs, near(d), c).wait_send()
+                if far:
+                    zz_copy(k, near(d), c).wait_send()
+            loop(1, half, sent)
+            if far:
+                z_copy(k, fs, mirror, c).wait_send()
+
+            def sent2(a2):
+                y_copy(k, 2 * a2 + b, c).wait_send()
+            loop(0, na, sent2)
 
     barrier = pltpu.get_barrier_semaphore()
 
@@ -306,6 +364,22 @@
         pl.semaphore_signal(barrier, inc=1, device_id=dev(g, fs, tp), device_id_type=MESH)
     cast_w(0, 0)
     pl.semaphore_wait(barrier, n + T + G - 3)
+
+    def norm_rows(j):
+        p[0, j] = normed_of(prompt[j].astype(f32))
+
+    def start_tokens():
+        loop(0, n, norm_rows)
+        flatten(p.at[0])
+        st[...] = prompt[fs].astype(f32)
+
+    def unpack(k):
+        flatten(ag.at[k])
+
+    def done(k):
+        gather_done(k)
+        rs_done(k)
+        ag_done(k)
 
     xsend_w(0, 0)
     plane_own(0, 0)
@@ -317,48 +391,65 @@
     cast_w(1, 0)
     cast_w(1, 1)
     cast_d(1)
-
-    def norm_rows(j):
-        p[0, j] = normed_of(prompt[j].astype(f32))
-    loop(0, n, norm_rows)
-    flatten(p.at[0])
-    st[...] = prompt[fs].astype(f32)
-
+    start_tokens()
+    xsend_w(1, 0)
     plane_x(0, 0)
     plane_x(0, 1)
-    xsend_w(1, 0)
     plane_own(1, 0)
+    arrive(0, 0)
     xsend_w(1, 1)
     plane_x(1, 0)
     plane_own(1, 1)
+    arrive(0, 1)
+    relay_d(0)
+    cross(0, 0)
+    cross(0, 1)
+    landed(0, 0)
+    landed(0, 1)
     plane_x(1, 1)
-    gather_w(0, 0)
-    gather_w(0, 1)
     xsend_d(1)
-    gather_d(0)
+    landed_d(0)
     compute(0)
     rs_first(0)
-    rs_second(0)
-    rs_last(0)
-    ag[0, fs] = normed_of(st[...])
-    ag_start(0)
-    gather_w(1, 0)
-    ag_rest(0)
-    flatten(ag.at[0])
-    gather_w(1, 1)
-    gather_d(1)
+    arrive(1, 0)
+    rs_remote(0, 0)
+    rs_own(0, 0)
+    if C > 1:
+        rs_remote(0, 1)
+    if C > 1:
+        rs_last(0, 0)
+    if C > 1:
+        rs_own(0, 1)
+    arrive(1, 1)
+    rs_last(0, C - 1)
+    relay_d(1)
+    ag_relay(0, 0)
+    cross(1, 0)
+    if C > 1:
+        ag_relay(0, 1)
+    ag_take(0)
+    unpack(0)
+    cross(1, 1)
+    landed(1, 0)
+    landed(1, 1)
+    landed_d(1)
     compute(1)
     rs_first(1)
-    rs_second(1)
-    rs_last(1)
-    ag[1, fs] = st[...].astype(bf16)
-    ag_start(1)
-    ag_rest(1)
-    for k in range(2):
-        gather_done(k)
-        rs_done(k)
-        ag_done(k)
-
+    rs_remote(1, 0)
+    rs_own(1, 0)
+    if C > 1:
+        rs_remote(1, 1)
+    if C > 1:
+        rs_last(1, 0)
+    if C > 1:
+        rs_own(1, 1)
+    rs_last(1, C - 1)
+    ag_relay(1, 0)
+    if C > 1:
+        ag_relay(1, 1)
+    ag_take(1)
+    done(0)
+    done(1)
 
 def write_out(wall, dn, ag, gate_o, up_o, down_o, mixed_o, o_s, d_s, m_s):
     L, S, _, DC = dn.shape
@@ -384,6 +475,7 @@
     q = C // FFb
     tb = rows // n
     na = n // 2
+    C = max(1, min(2, tb // 8))
     dma = pltpu.SemaphoreType.DMA
     vmem = pl.BlockSpec(memory_space=pltpu.VMEM)
     anym = pl.BlockSpec(memory_space=pl.ANY)
@@ -408,8 +500,8 @@
             dma((L, 2, q, G)), dma((L, 2, q, G)), dma((L, 2, n)), dma((L, 2, 2, n)), dma((L, G)),
             dma((L, 2, G, q)), dma((L, 2, n)), dma((L, 2)), dma((L, 2, 2, n, T)),
             dma((L, G, T)), dma((L, G * T)),
-            dma((L, na)), dma((L, na)), dma((L, na)), dma((L, na)),
-            dma((L, na)), dma((L, n)), dma((L, na)),
+            dma((L, na, C)), dma((L, na, C)), dma((L, na, C)), dma((L, na, C)),
+            dma((L, na, C)), dma((L, na, C)), dma((L, n, C)), dma((L, na, C)),
         ],
         compiler_params=pltpu.CompilerParams(
             collective_id=0, has_side_effects=True, vmem_limit_bytes=40 * 1024 * 1024),

time: 178 us -> 148 us (0.83)
  Pallas kernels: 175 us -> 146 us
    pallas_call x1, Pallas kernels: 170 us -> 141 us  [per_device(): pl.pallas_call(functools.partial(kernel, G, n, T), out_shape=(pltpu.VMEM(...]
where the time goes in v1:
time: 148 us
  Pallas kernels  146 us (99%)
  local copies, waits for them, and re-layouts  1.53 us (1%)
    pallas_call x1, Pallas kernels, per_device(): pl.pallas_call(functools.partial(kernel, G, n, T), out_shape=(pltpu.VMEM(...  141 us
    pallas_call x1, Pallas kernels, per_device(): pl.pallas_call(write_out, out_shape=(jax.ShapeDtypeStruct((L, n, R, FFb),...  4.99 us

profile of v1, /device:TPU:0, one launch (start us, length us, event | category | flops | bytes accessed | tf_op | source)
XLA Modules:
  0.0 147.9 jit_solution(9352455576751825240)
XLA Ops:
  0.6 1.5 %copy.9.gain = f32[2,256,1]{2,1,0:T(8,128)} copy(f32[2,256,1]{1,0,2:T(2,128)} %bitcast.6) | data formatting | bytes 4096 | tf_op jit(solution)/shard_map/broadcast_in_dim | solution.py:508
  2.2 140.7 %shard_map.84 = (bf16[2,2,8,256,512]{4,3,2,1,0:T(8,128)(2,1)S(1)}, bf16[2,4,512,512]{3,2,1,0:T(8,128)(2,1)S(1)}, bf16[2,8,32,2048]{3,2,1,0:T(8,128)(2,1)S(1)}) custom-call(bf16[8,32,2048]{2,1,0:T(8,128)(2,1)} %bitcast.5, f32[2,256,1]{2,1,0:T(8,128)} %copy.9.gain, f32[2,256,1024]{2,1,0:T(8,128)} %gate_w.1, f32[2,256,1024]{2,1,0:T(8,128)} %up_w.1, ...), custom_call_target="tpu_custom_call" | custom-call | tf_op jit(solution)/shard_map/pallas_call | solution.py:482
  142.9 5.0 %shard_map.85 = (bf16[2,8,256,512]{3,2,1,0:T(8,128)(2,1)}, bf16[2,8,256,512]{3,2,1,0:T(8,128)(2,1)}, bf16[2,512,2048]{2,1,0:T(8,128)(2,1)}, bf16[8,32,2048]{2,1,0:T(8,128)(2,1)}) custom-call(bf16[2,2,8,256,512]{4,3,2,1,0:T(8,128)(2,1)S(1)} %get-tuple-element.11.wall, bf16[2,4,512,512]{3,2,1,0:T(8,128)(2,1)S(1)} %get-tuple-element.12.dn, ...), custom_call_target="tpu_custom_call" | custom-call | tf_op jit(solution)/shard_map/pallas_call | solution.py:509

commit v2 on v1

--- a/solution.py
+++ b/solution.py
@@ -13,17 +13,18 @@
 bf16 = jnp.bfloat16
 
 
-def kernel(G, n, T, prompt, gain, gate_w, up_w, down_w,
+def kernel(G, n, T, prompt_h, gain_h, gate_h, up_h, down_h,
            wall, dn, ag,
-           wsrc, p, r1, q2, r2, lhs, hid, st,
+           prompt, gain, gate_w, up_w, down_w, in_s, wsrc, p, r1, q2, r2, r3, sums, lhs, hid, st,
            x_s, x_r, v_s, v_r, xd_s, p_s, w_r, w_l, f_s, d_s, d_r,
-           s1_s, s1_r, s2_s, s2_r, g_s, gg_s, g_r, h_s):
+           s1_s, s1_r, s2_s, s2_r, s3_s, s3_r, g_s, gg_s, g_r, h_s):
     gr, fs, tp = lax.axis_index("gr"), lax.axis_index("fs"), lax.axis_index("tp")
     q, R, FFb = wsrc.shape[3:]
     tb, D = prompt.shape[1:]
     rows = n * tb
     DC = dn.shape[3]
     na = n // 2
+    wing = n // 2 if n % 2 == 0 else n
     a, b = fs // 2, lax.rem(fs, 2)
     C = s1_s.shape[2]
     tc = tb // C
@@ -52,7 +53,13 @@
             return c
         lax.fori_loop(lo, hi, step, 0)
 
+    turn = [lax.rem(i + b + 1, q) for i in range(q)]
     others_g = [lax.rem(gr + d, G) for d in range(1, G)]
+    loads = [pltpu.make_async_copy(gain_h, gain, in_s.at[0])]
+    for k in range(2):
+        for h, v in ((gate_h, gate_w), (up_h, up_w), (down_h, down_w)):
+            loads.append(pltpu.make_async_copy(h.at[k], v.at[k], in_s.at[len(loads)]))
+    loads.append(pltpu.make_async_copy(prompt_h, prompt, in_s.at[len(loads)]))
     others_t = [lax.rem(tp + d, T) for d in range(1, T)]
 
     def x_copy(k, w, i, g_src, g_dst):
@@ -89,17 +96,23 @@
         blk = wall.at[k, w, f, only(k, 1 - gr)]
         return rc(blk, blk, f_s.at[k, w, 1, f, t], v_r.at[k, w, 1, f], dev(gr, fs, t))
 
+    def column(k):
+        eye = lax.broadcasted_iota(jnp.int32, (R, R), 0) == lax.broadcasted_iota(jnp.int32, (R, R), 1)
+        return jnp.sum(jnp.where(eye, gain[k:k + 1], 0.0), axis=1, keepdims=True)
+
     def cast_w(k, w):
         ref = (gate_w, up_w)[w]
+        loads[1 + 3 * k + w].wait()
         for i in range(q):
-            wsrc[k, w, gr, i] = (gain[k] * ref[k, :, i * FFb:(i + 1) * FFb]).astype(bf16)
+            wsrc[k, w, gr, i] = (column(k) * ref[k, :, i * FFb:(i + 1) * FFb]).astype(bf16)
 
     def xsend_w(k, w):
-        for i in range(q):
+        for i in turn:
             for g in others_g:
                 x_copy(k, w, i, gr, g).start()
 
     def cast_d(k):
+        loads[3 + 3 * k].wait()
         dn[k, slot_me] = down_w[k].astype(bf16)
 
     def xsend_d(k):
@@ -120,14 +133,18 @@
             l_copy(k, w, g, i).start()
 
     def plane_own(k, w):
-        for i in range(q):
+        for i in turn:
             plane(k, w, gr, i)
 
     def plane_x(k, w):
         for g in others_g:
-            for i in range(q):
+            for i in turn:
                 x_copy(k, w, i, g, gr).wait_recv()
                 plane(k, w, g, i)
+
+    def source(s):
+        e = s // wing
+        return lax.rem((fs // wing + e) * wing + lax.rem(fs + s, wing), n)
 
     def arrive(k, w):
         def forward(f):
@@ -142,7 +159,7 @@
             forward(fs)
 
             def take(s):
-                f = lax.rem(fs + s, n)
+                f = source(s)
                 f_copy(k, w, f, tp).wait_recv()
                 forward(f)
             loop(1, n, take)
@@ -152,7 +169,7 @@
             @pl.when(is_recv)
             def _():
                 def take(s):
-                    f = lax.rem(fs + s, n)
+                    f = source(s)
                     v_copy(k, w, f, 1 - gr).wait_recv()
                     for t in others_t:
                         fv_copy(k, w, f, t).start()
@@ -240,9 +257,8 @@
     def near(d):
         return a - pos + lax.rem(pos + d, half)
 
-    def partner(d):
-        e = lax.div(d, half) if far else 1
-        return lax.rem(a // half + 1 - e, far + 1) * half + lax.rem(pos + d + (e if far else 1), half)
+    def across(a2):
+        return lax.rem(a2 + half, na)
 
     def part(c):
         return pl.ds(c * tc, tc)
@@ -255,31 +271,64 @@
         return rc(q2.at[k, a2, part(c)], r2.at[k, a_from, part(c)],
                   s2_s.at[k, a2, c], s2_r.at[k, a_from, c], dev(gr, 2 * a2 + b, tp))
 
+    def s3_copy(k, o, a_from, c):
+        return rc(q2.at[k, across(o), part(c)], r3.at[k, a_from, part(c)],
+                  s3_s.at[k, o, c], s3_r.at[k, a_from, c], dev(gr, 2 * o + b, tp))
+
     def rs_first(k):
         for c in range(C):
+            if far:
+                def send_far(d):
+                    s1_copy(k, across(near(d)), c).start()
+                loop(1, half, send_far)
+
             def send(d):
-                s1_copy(k, partner(d), c).start()
-            loop(0, na - 1, send)
+                s1_copy(k, near(d), c).start()
+            loop(1, half, send)
+            if far:
+                s1_copy(k, mirror, c).start()
             s1_copy(k, a, c).start()
 
+    def pair(k, a2, c):
+        s1_copy(k, a2, c).wait_recv()
+        return p[k, 2 * a2 + b, part(c)].astype(f32) + r1[k, a2, part(c)].astype(f32)
+
     def rs_remote(k, c):
+        if far:
+            def help_far(d):
+                o = near(d)
+                q2[k, across(o), part(c)] = pair(k, across(o), c).astype(bf16)
+                s3_copy(k, o, a, c).start()
+            loop(1, half, help_far)
+
         def send(d):
-            a2 = partner(d)
-            s1_copy(k, a2, c).wait_recv()
-            q2[k, a2, part(c)] = (p[k, 2 * a2 + b, part(c)].astype(f32) + r1[k, a2, part(c)].astype(f32)).astype(bf16)
-            s2_copy(k, a2, a, c).start()
-        loop(0, na - 1, send)
+            o = near(d)
+            q2[k, o, part(c)] = pair(k, o, c).astype(bf16)
+            s2_copy(k, o, a, c).start()
+        loop(1, half, send)
+
+    def rs_mid(k, c):
+        if far:
+            sums[part(c)] = pair(k, mirror, c)
+
+            def take(d):
+                o = near(d)
+                s3_copy(k, a, o, c).wait_recv()
+                sums[part(c)] += r3[k, o, part(c)].astype(f32)
+            loop(1, half, take)
+            q2[k, mirror, part(c)] = sums[part(c)].astype(bf16)
+            s2_copy(k, mirror, a, c).start()
 
     def rs_own(k, c):
-        s1_copy(k, a, c).wait_recv()
-        st[part(c)] += 0.5 * (p[k, fs, part(c)].astype(f32) + r1[k, a, part(c)].astype(f32))
+        st[part(c)] += 0.5 * pair(k, a, c)
 
     def rs_last(k, c):
-        def take(d):
-            a2 = partner(na - 2 - d)
+        def take(a2):
             s2_copy(k, a2, a2, c).wait_recv()
             st[part(c)] += 0.5 * r2[k, a2, part(c)].astype(f32)
-        loop(0, na - 1, take)
+        loop(1, half, lambda d: take(near(d)))
+        if far:
+            take(mirror)
         x = st[part(c)]
         ag[k, fs, part(c)] = normed_of(x) if k == 0 else x.astype(bf16)
 
@@ -303,13 +352,13 @@
         blk = ag.at[k, 2 * mirror + b, part(c)]
         return rc(blk, blk, gg_s.at[k, a2, c], g_r.at[k, 2 * mirror + b, c], dev(gr, 2 * a2 + b, tp))
 
-    def ag_relay(k, c):
-        def pass_on(a2):
-            z_copy(k, 2 * a2 + b, a2, c).wait_recv()
-            y_copy(k, 2 * a2 + b, c).start()
-
+    def pass_on(k, a2, c):
+        z_copy(k, 2 * a2 + b, a2, c).wait_recv()
+        y_copy(k, 2 * a2 + b, c).start()
+
+    def ag_pass(k, c):
         def own(d):
-            pass_on(near(d))
+            pass_on(k, near(d), c)
         loop(1, half, own)
         if far:
             z_copy(k, 2 * mirror + b, a, c).wait_recv()
@@ -319,8 +368,10 @@
             loop(1, half, spread)
             y_copy(k, 2 * mirror + b, c).start()
 
+    def ag_far(k, c):
+        if far:
             def theirs(d):
-                pass_on(lax.rem(near(d) + half, na))
+                pass_on(k, across(near(d)), c)
             loop(1, half, theirs)
 
     def ag_take(k):
@@ -336,8 +387,12 @@
             loop(0, na, sent)
 
             def sent2(d):
-                s2_copy(k, partner(d), a, c).wait_send()
-            loop(0, na - 1, sent2)
+                s2_copy(k, near(d), a, c).wait_send()
+                if far:
+                    s3_copy(k, near(d), a, c).wait_send()
+            loop(1, half, sent2)
+            if far:
+                s2_copy(k, mirror, a, c).wait_send()
 
     def ag_done(k):
         for c in range(C):
@@ -353,6 +408,8 @@
                 y_copy(k, 2 * a2 + b, c).wait_send()
             loop(0, na, sent2)
 
+    for load in loads:
+        load.start()
     barrier = pltpu.get_barrier_semaphore()
 
     def greet(s):
@@ -362,6 +419,7 @@
         pl.semaphore_signal(barrier, inc=1, device_id=dev(gr, fs, t), device_id_type=MESH)
     for g in others_g:
         pl.semaphore_signal(barrier, inc=1, device_id=dev(g, fs, tp), device_id_type=MESH)
+    loads[0].wait()
     cast_w(0, 0)
     pl.semaphore_wait(barrier, n + T + G - 3)
 
@@ -369,6 +427,7 @@
         p[0, j] = normed_of(prompt[j].astype(f32))
 
     def start_tokens():
+        loads[7].wait()
         loop(0, n, norm_rows)
         flatten(p.at[0])
         st[...] = prompt[fs].astype(f32)
@@ -395,61 +454,68 @@
     xsend_w(1, 0)
     plane_x(0, 0)
     plane_x(0, 1)
-    plane_own(1, 0)
     arrive(0, 0)
-    xsend_w(1, 1)
-    plane_x(1, 0)
-    plane_own(1, 1)
     arrive(0, 1)
     relay_d(0)
     cross(0, 0)
+    landed(0, 0)
+    xsend_w(1, 1)
+    plane_own(1, 0)
+    plane_x(1, 0)
     cross(0, 1)
-    landed(0, 0)
     landed(0, 1)
-    plane_x(1, 1)
-    xsend_d(1)
+    plane_own(1, 1)
     landed_d(0)
     compute(0)
     rs_first(0)
+    plane_x(1, 1)
+    xsend_d(1)
+    rs_remote(0, 0)
     arrive(1, 0)
-    rs_remote(0, 0)
+    rs_mid(0, 0)
     rs_own(0, 0)
     if C > 1:
         rs_remote(0, 1)
-    if C > 1:
         rs_last(0, 0)
-    if C > 1:
+        rs_mid(0, 1)
         rs_own(0, 1)
     arrive(1, 1)
     rs_last(0, C - 1)
     relay_d(1)
-    ag_relay(0, 0)
+    ag_pass(0, 0)
+    ag_far(0, 0)
+    if C > 1:
+        ag_pass(0, 1)
+        ag_far(0, 1)
     cross(1, 0)
-    if C > 1:
-        ag_relay(0, 1)
+    cross(1, 1)
     ag_take(0)
     unpack(0)
-    cross(1, 1)
     landed(1, 0)
     landed(1, 1)
     landed_d(1)
     compute(1)
     rs_first(1)
     rs_remote(1, 0)
+    rs_mid(1, 0)
     rs_own(1, 0)
     if C > 1:
         rs_remote(1, 1)
+        rs_last(1, 0)
+        rs_mid(1, 1)
+        rs_own(1, 1)
+        ag_pass(1, 0)
+    rs_last(1, C - 1)
+    if C == 1:
+        ag_pass(1, 0)
+    ag_far(1, 0)
     if C > 1:
-        rs_last(1, 0)
-    if C > 1:
-        rs_own(1, 1)
-    rs_last(1, C - 1)
-    ag_relay(1, 0)
-    if C > 1:
-        ag_relay(1, 1)
+        ag_pass(1, 1)
+        ag_far(1, 1)
     ag_take(1)
     done(0)
     done(1)
+
 
 def write_out(wall, dn, ag, gate_o, up_o, down_o, mixed_o, o_s, d_s, m_s):
     L, S, _, DC = dn.shape
@@ -470,9 +536,9 @@
 def per_device(G, n, T, prompt, norm_gain, gate_weight, up_weight, down_weight):
     D = prompt.shape[2]
     rows = prompt.shape[0] * prompt.shape[1]
-    L, R, C = gate_weight.shape
+    L, R, C_ = gate_weight.shape
     FFb, DC = down_weight.shape[1:]
-    q = C // FFb
+    q = C_ // FFb
     tb = rows // n
     na = n // 2
     C = max(1, min(2, tb // 8))
@@ -486,26 +552,31 @@
             pltpu.VMEM((L, G * T, FFb, DC), bf16),
             pltpu.VMEM((L, n, tb, D), bf16),
         ),
-        in_specs=[vmem] * 5,
+        in_specs=[pl.BlockSpec(memory_space=pltpu.HBM)] * 5,
         out_specs=(vmem,) * 3,
         scratch_shapes=[
+            pltpu.VMEM((n, tb, D), bf16), pltpu.VMEM((L, R), f32),
+            pltpu.VMEM((L, R, C_), f32), pltpu.VMEM((L, R, C_), f32), pltpu.VMEM((L, FFb, DC), f32),
+            dma((8,)),
             pltpu.VMEM((L, 2, G, q, R, FFb), bf16),
             pltpu.VMEM((L, n, tb, D), bf16),
             pltpu.VMEM((L, na, tb, D), bf16),
             pltpu.VMEM((L, na, tb, D), bf16),
             pltpu.VMEM((L, na, tb, D), bf16),
+            pltpu.VMEM((L, na, tb, D), bf16),
+            pltpu.VMEM((tb, D), f32),
             pltpu.VMEM((rows, D), bf16),
             pltpu.VMEM((rows, FFb), bf16),
             pltpu.VMEM((tb, D), f32),
             dma((L, 2, q, G)), dma((L, 2, q, G)), dma((L, 2, n)), dma((L, 2, 2, n)), dma((L, G)),
             dma((L, 2, G, q)), dma((L, 2, n)), dma((L, 2)), dma((L, 2, 2, n, T)),
             dma((L, G, T)), dma((L, G * T)),
-            dma((L, na, C)), dma((L, na, C)), dma((L, na, C)), dma((L, na, C)),
+            dma((L, na, C)), dma((L, na, C)), dma((L, na, C)), dma((L, na, C)), dma((L, na, C)), dma((L, na, C)),
             dma((L, na, C)), dma((L, na, C)), dma((L, n, C)), dma((L, na, C)),
         ],
         compiler_params=pltpu.CompilerParams(
             collective_id=0, has_side_effects=True, vmem_limit_bytes=40 * 1024 * 1024),
-    )(prompt.reshape(n, tb, D), norm_gain[:, :, None], gate_weight, up_weight, down_weight)
+    )(prompt.reshape(n, tb, D), norm_gain, gate_weight, up_weight, down_weight)
     gate, up, down, mixed = pl.pallas_call(
         write_out,
         out_shape=(

time: 148 us -> 138 us (0.932)
  Pallas kernels: 146 us -> 137 us
  local copies, waits for them, and re-layouts: 1.53 us -> 0 us
    pallas_call x1, Pallas kernels: 141 us -> 132 us  [per_device(): pl.pallas_call(functools.partial(kernel, G, n, T), out_shape=(pltpu.VMEM(...]
    broadcast_in_dim x1 -> x0, local copies, waits for them, and re-layouts: 1.53 us -> none  [per_device(): norm_gain[:, :, None]]
where the time goes in v2:
time: 138 us
  Pallas kernels  137 us (99%)
    pallas_call x1, Pallas kernels, per_device(): pl.pallas_call(functools.partial(kernel, G, n, T), out_shape=(pltpu.VMEM(...  132 us
    pallas_call x1, Pallas kernels, per_device(): pl.pallas_call(write_out, out_shape=(jax.ShapeDtypeStruct((L, n, R, FFb),...  4.99 us

profile of v2, /device:TPU:0, one launch (start us, length us, event | category | flops | bytes accessed | tf_op | source)
XLA Modules:
  0.0 138.1 jit_solution(2353522478044848601)
XLA Ops:
  0.6 132.5 %shard_map.84 = (bf16[2,2,8,256,512]{4,3,2,1,0:T(8,128)(2,1)S(1)}, bf16[2,4,512,512]{3,2,1,0:T(8,128)(2,1)S(1)}, bf16[2,8,32,2048]{3,2,1,0:T(8,128)(2,1)S(1)}) custom-call(bf16[8,32,2048]{2,1,0:T(8,128)(2,1)} %bitcast.4, f32[2,256]{1,0:T(2,128)} %gain_h.1, f32[2,256,1024]{2,1,0:T(8,128)} %gate_h.1, f32[2,256,1024]{2,1,0:T(8,128)} %up_h.1, f32[2,512,512]{2,1,0:T(8,128)} %down_h.1), custom_call_target="tpu_custom_call" | custom-call | tf_op jit(solution)/shard_map/pallas_call | solution.py:548
  133.1 5.0 %shard_map.85 = (bf16[2,8,256,512]{3,2,1,0:T(8,128)(2,1)}, bf16[2,8,256,512]{3,2,1,0:T(8,128)(2,1)}, bf16[2,512,2048]{2,1,0:T(8,128)(2,1)}, bf16[8,32,2048]{2,1,0:T(8,128)(2,1)}) custom-call(bf16[2,2,8,256,512]{4,3,2,1,0:T(8,128)(2,1)S(1)} %get-tuple-element.11.wall, bf16[2,4,512,512]{3,2,1,0:T(8,128)(2,1)S(1)} %get-tuple-element.12.dn, ...), custom_call_target="tpu_custom_call" | custom-call | tf_op jit(solution)/shard_map/pallas_call | solution.py:580

commit v3 on v2

--- a/solution.py
+++ b/solution.py
@@ -15,7 +15,7 @@
 
 def kernel(G, n, T, prompt_h, gain_h, gate_h, up_h, down_h,
            wall, dn, ag,
-           prompt, gain, gate_w, up_w, down_w, in_s, wsrc, p, r1, q2, r2, r3, sums, lhs, hid, st,
+           prompt, gain, gate_w, up_w, down_w, in_s, wsrc, p, r1, q2, r2, r3, sums, lhs, hid, gact, st,
            x_s, x_r, v_s, v_r, xd_s, p_s, w_r, w_l, f_s, d_s, d_r,
            s1_s, s1_r, s2_s, s2_r, s3_s, s3_r, g_s, gg_s, g_r, h_s):
     gr, fs, tp = lax.axis_index("gr"), lax.axis_index("fs"), lax.axis_index("tp")
@@ -233,21 +233,32 @@
     def normed_of(x):
         return (x * lax.rsqrt(jnp.mean(x * x, axis=-1, keepdims=True) + norm_eps)).astype(bf16)
 
+    def gates(k):
+        ft = min(FFb, 256)
+
+        def act(j):
+            cols = pl.ds(j * ft, ft)
+            gact[:, cols] = jnp.dot(lhs[...], wall[k, 0, :, :, cols].reshape(D, ft), preferred_element_type=f32)
+        for j in range(FFb // ft):
+            act(j)
+
     def compute(k):
         ft = min(FFb, 256)
 
         def act(j):
-            cols = pl.ds(pl.multiple_of(j * ft, ft), ft)
-            gate = jnp.dot(lhs[...], wall[k, 0, :, :, cols].reshape(D, ft), preferred_element_type=f32)
+            cols = pl.ds(j * ft, ft)
+            gate = gact[:, cols]
             up = jnp.dot(lhs[...], wall[k, 1, :, :, cols].reshape(D, ft), preferred_element_type=f32)
             hid[:, cols] = (gate / (1.0 + jnp.exp(-gate)) * up).astype(bf16)
-        loop(0, FFb // ft, act)
+        for j in range(FFb // ft):
+            act(j)
 
         def proj(s):
-            cols = pl.ds(pl.multiple_of(s * DC, DC), DC)
+            cols = pl.ds(s * DC, DC)
             v = jnp.dot(hid[...], dn[k, s], preferred_element_type=f32)
             p[k, :, :, cols] = v.reshape(n, tb, DC).astype(bf16)
-        loop(0, G * T, proj)
+        for s in range(G * T):
+            proj(s)
 
     half = na // 2 if na % 2 == 0 else na
     far = na // half - 1
@@ -276,31 +287,30 @@
                   s3_s.at[k, o, c], s3_r.at[k, a_from, c], dev(gr, 2 * o + b, tp))
 
     def rs_first(k):
-        for c in range(C):
-            if far:
-                def send_far(d):
-                    s1_copy(k, across(near(d)), c).start()
-                loop(1, half, send_far)
-
-            def send(d):
-                s1_copy(k, near(d), c).start()
-            loop(1, half, send)
-            if far:
-                s1_copy(k, mirror, c).start()
-            s1_copy(k, a, c).start()
+        def send(of):
+            def chunks(d):
+                for c in range(C):
+                    s1_copy(k, of(d), c).start()
+            return chunks
+        if far:
+            loop(1, half, send(lambda d: across(near(d))))
+            send(lambda d: mirror)(0)
+        loop(1, half, send(near))
+        send(lambda d: a)(0)
 
     def pair(k, a2, c):
         s1_copy(k, a2, c).wait_recv()
         return p[k, 2 * a2 + b, part(c)].astype(f32) + r1[k, a2, part(c)].astype(f32)
 
-    def rs_remote(k, c):
+    def rs_far(k, c):
         if far:
-            def help_far(d):
+            def send(d):
                 o = near(d)
                 q2[k, across(o), part(c)] = pair(k, across(o), c).astype(bf16)
                 s3_copy(k, o, a, c).start()
-            loop(1, half, help_far)
-
+            loop(1, half, send)
+
+    def rs_near(k, c):
         def send(d):
             o = near(d)
             q2[k, o, part(c)] = pair(k, o, c).astype(bf16)
@@ -462,6 +472,7 @@
     xsend_w(1, 1)
     plane_own(1, 0)
     plane_x(1, 0)
+    gates(0)
     cross(0, 1)
     landed(0, 1)
     plane_own(1, 1)
@@ -470,47 +481,58 @@
     rs_first(0)
     plane_x(1, 1)
     xsend_d(1)
-    rs_remote(0, 0)
+    rs_far(0, 0)
+    if C > 1:
+        rs_far(0, 1)
     arrive(1, 0)
     rs_mid(0, 0)
+    if C > 1:
+        rs_mid(0, 1)
+    rs_near(0, 0)
+    if C > 1:
+        rs_near(0, 1)
     rs_own(0, 0)
     if C > 1:
-        rs_remote(0, 1)
         rs_last(0, 0)
-        rs_mid(0, 1)
         rs_own(0, 1)
     arrive(1, 1)
     rs_last(0, C - 1)
     relay_d(1)
     ag_pass(0, 0)
+    if C > 1:
+        ag_pass(0, 1)
     ag_far(0, 0)
     if C > 1:
-        ag_pass(0, 1)
         ag_far(0, 1)
     cross(1, 0)
-    cross(1, 1)
     ag_take(0)
     unpack(0)
     landed(1, 0)
+    gates(1)
+    cross(1, 1)
     landed(1, 1)
     landed_d(1)
     compute(1)
     rs_first(1)
-    rs_remote(1, 0)
+    rs_far(1, 0)
+    if C > 1:
+        rs_far(1, 1)
     rs_mid(1, 0)
+    if C > 1:
+        rs_mid(1, 1)
+    rs_near(1, 0)
+    if C > 1:
+        rs_near(1, 1)
     rs_own(1, 0)
     if C > 1:
-        rs_remote(1, 1)
         rs_last(1, 0)
-        rs_mid(1, 1)
         rs_own(1, 1)
-        ag_pass(1, 0)
     rs_last(1, C - 1)
-    if C == 1:
-        ag_pass(1, 0)
+    ag_pass(1, 0)
+    if C > 1:
+        ag_pass(1, 1)
     ag_far(1, 0)
     if C > 1:
-        ag_pass(1, 1)
         ag_far(1, 1)
     ag_take(1)
     done(0)
@@ -567,6 +589,7 @@
             pltpu.VMEM((tb, D), f32),
             pltpu.VMEM((rows, D), bf16),
             pltpu.VMEM((rows, FFb), bf16),
+            pltpu.VMEM((rows, FFb), f32),
             pltpu.VMEM((tb, D), f32),
             dma((L, 2, q, G)), dma((L, 2, q, G)), dma((L, 2, n)), dma((L, 2, 2, n)), dma((L, G)),
             dma((L, 2, G, q)), dma((L, 2, n)), dma((L, 2)), dma((L, 2, 2, n, T)),

time: 138 us -> 136 us (0.986)
  Pallas kernels: 137 us -> 135 us
    pallas_call x1, Pallas kernels: 132 us -> 130 us  [per_device(): pl.pallas_call(functools.partial(kernel, G, n, T), out_shape=(pltpu.VMEM(...]
where the time goes in v3:
time: 136 us
  Pallas kernels  135 us (99%)
    pallas_call x1, Pallas kernels, per_device(): pl.pallas_call(functools.partial(kernel, G, n, T), out_shape=(pltpu.VMEM(...  130 us
    pallas_call x1, Pallas kernels, per_device(): pl.pallas_call(write_out, out_shape=(jax.ShapeDtypeStruct((L, n, R, FFb),...  4.99 us

profile of v3, /device:TPU:0, one launch (start us, length us, event | category | flops | bytes accessed | tf_op | source)
XLA Modules:
  0.0 135.8 jit_solution(8905434198259781619)
XLA Ops:
  0.6 130.1 %shard_map.84 = (bf16[2,2,8,256,512]{4,3,2,1,0:T(8,128)(2,1)S(1)}, bf16[2,4,512,512]{3,2,1,0:T(8,128)(2,1)S(1)}, bf16[2,8,32,2048]{3,2,1,0:T(8,128)(2,1)S(1)}) custom-call(bf16[8,32,2048]{2,1,0:T(8,128)(2,1)} %bitcast.4, f32[2,256]{1,0:T(2,128)} %gain_h.1, f32[2,256,1024]{2,1,0:T(8,128)} %gate_h.1, f32[2,256,1024]{2,1,0:T(8,128)} %up_h.1, f32[2,512,512]{2,1,0:T(8,128)} %down_h.1), custom_call_target="tpu_custom_call" | custom-call | tf_op jit(solution)/shard_map/pallas_call | solution.py:570
  130.8 5.0 %shard_map.85 = (bf16[2,8,256,512]{3,2,1,0:T(8,128)(2,1)}, bf16[2,8,256,512]{3,2,1,0:T(8,128)(2,1)}, bf16[2,512,2048]{2,1,0:T(8,128)(2,1)}, bf16[8,32,2048]{2,1,0:T(8,128)(2,1)}) custom-call(bf16[2,2,8,256,512]{4,3,2,1,0:T(8,128)(2,1)S(1)} %get-tuple-element.11.wall, bf16[2,4,512,512]{3,2,1,0:T(8,128)(2,1)S(1)} %get-tuple-element.12.dn, ...), custom_call_target="tpu_custom_call" | custom-call | tf_op jit(solution)/shard_map/pallas_call | solution.py:603

commit v4 on v3

--- a/solution.py
+++ b/solution.py
@@ -15,7 +15,7 @@
 
 def kernel(G, n, T, prompt_h, gain_h, gate_h, up_h, down_h,
            wall, dn, ag,
-           prompt, gain, gate_w, up_w, down_w, in_s, wsrc, p, r1, q2, r2, r3, sums, lhs, hid, gact, st,
+           prompt, gain, gate_w, up_w, down_w, in_s, wsrc, p, r1, q2, r2, r3, sums, hid, gact, st,
            x_s, x_r, v_s, v_r, xd_s, p_s, w_r, w_l, f_s, d_s, d_r,
            s1_s, s1_r, s2_s, s2_r, s3_s, s3_r, g_s, gg_s, g_r, h_s):
     gr, fs, tp = lax.axis_index("gr"), lax.axis_index("fs"), lax.axis_index("tp")
@@ -222,13 +222,8 @@
             for t in others_t:
                 d_copy(k, g, tp, t).wait_send()
 
-    def flatten(ref):
-        cw = 256
-
-        def chunk(j):
-            cols = pl.ds(pl.multiple_of(j * cw, cw), cw)
-            lhs[:, cols] = ref[:, :, cols].astype(f32).reshape(rows, cw).astype(bf16)
-        loop(0, D // cw, chunk)
+    def tokens(k):
+        return (p if k == 0 else ag)[0].reshape(rows, D)
 
     def normed_of(x):
         return (x * lax.rsqrt(jnp.mean(x * x, axis=-1, keepdims=True) + norm_eps)).astype(bf16)
@@ -238,7 +233,7 @@
 
         def act(j):
             cols = pl.ds(j * ft, ft)
-            gact[:, cols] = jnp.dot(lhs[...], wall[k, 0, :, :, cols].reshape(D, ft), preferred_element_type=f32)
+            gact[:, cols] = jnp.dot(tokens(k), wall[k, 0, :, :, cols].reshape(D, ft), preferred_element_type=f32)
         for j in range(FFb // ft):
             act(j)
 
@@ -248,7 +243,7 @@
         def act(j):
             cols = pl.ds(j * ft, ft)
             gate = gact[:, cols]
-            up = jnp.dot(lhs[...], wall[k, 1, :, :, cols].reshape(D, ft), preferred_element_type=f32)
+            up = jnp.dot(tokens(k), wall[k, 1, :, :, cols].reshape(D, ft), preferred_element_type=f32)
             hid[:, cols] = (gate / (1.0 + jnp.exp(-gate)) * up).astype(bf16)
         for j in range(FFb // ft):
             act(j)
@@ -439,11 +434,7 @@
     def start_tokens():
         loads[7].wait()
         loop(0, n, norm_rows)
-        flatten(p.at[0])
         st[...] = prompt[fs].astype(f32)
-
-    def unpack(k):
-        flatten(ag.at[k])
 
     def done(k):
         gather_done(k)
@@ -506,7 +497,6 @@
         ag_far(0, 1)
     cross(1, 0)
     ag_take(0)
-    unpack(0)
     landed(1, 0)
     gates(1)
     cross(1, 1)
@@ -514,6 +504,7 @@
     landed_d(1)
     compute(1)
     rs_first(1)
+    done(0)
     rs_far(1, 0)
     if C > 1:
         rs_far(1, 1)
@@ -534,9 +525,10 @@
     ag_far(1, 0)
     if C > 1:
         ag_far(1, 1)
+    gather_done(1)
+    rs_done(1)
     ag_take(1)
-    done(0)
-    done(1)
+    ag_done(1)
 
 
 def write_out(wall, dn, ag, gate_o, up_o, down_o, mixed_o, o_s, d_s, m_s):
@@ -587,7 +579,6 @@
             pltpu.VMEM((L, na, tb, D), bf16),
             pltpu.VMEM((L, na, tb, D), bf16),
             pltpu.VMEM((tb, D), f32),
-            pltpu.VMEM((rows, D), bf16),
             pltpu.VMEM((rows, FFb), bf16),
             pltpu.VMEM((rows, FFb), f32),
             pltpu.VMEM((tb, D), f32),

time: 136 us -> 135 us (level)
  no operation moved by 1% of the time
where the time goes in v4:
time: 135 us
  Pallas kernels  134 us (99%)
    pallas_call x1, Pallas kernels, per_device(): pl.pallas_call(functools.partial(kernel, G, n, T), out_shape=(pltpu.VMEM(...  129 us
    pallas_call x1, Pallas kernels, per_device(): pl.pallas_call(write_out, out_shape=(jax.ShapeDtypeStruct((L, n, R, FFb),...  4.99 us

profile of v4, /device:TPU:0, one launch (start us, length us, event | category | flops | bytes accessed | tf_op | source)
XLA Modules:
  0.0 135.0 jit_solution(17898031212050104371)
XLA Ops:
  0.6 129.3 %shard_map.84 = (bf16[2,2,8,256,512]{4,3,2,1,0:T(8,128)(2,1)S(1)}, bf16[2,4,512,512]{3,2,1,0:T(8,128)(2,1)S(1)}, bf16[2,8,32,2048]{3,2,1,0:T(8,128)(2,1)S(1)}) custom-call(bf16[8,32,2048]{2,1,0:T(8,128)(2,1)} %bitcast.4, f32[2,256]{1,0:T(2,128)} %gain_h.1, f32[2,256,1024]{2,1,0:T(8,128)} %gate_h.1, f32[2,256,1024]{2,1,0:T(8,128)} %up_h.1, f32[2,512,512]{2,1,0:T(8,128)} %down_h.1), custom_call_target="tpu_custom_call" | custom-call | tf_op jit(solution)/shard_map/pallas_call | solution.py:562
  130.0 5.0 %shard_map.85 = (bf16[2,8,256,512]{3,2,1,0:T(8,128)(2,1)}, bf16[2,8,256,512]{3,2,1,0:T(8,128)(2,1)}, bf16[2,512,2048]{2,1,0:T(8,128)(2,1)}, bf16[8,32,2048]{2,1,0:T(8,128)(2,1)}) custom-call(bf16[2,2,8,256,512]{4,3,2,1,0:T(8,128)(2,1)S(1)} %get-tuple-element.11.wall, bf16[2,4,512,512]{3,2,1,0:T(8,128)(2,1)S(1)} %get-tuple-element.12.dn, ...), custom_call_target="tpu_custom_call" | custom-call | tf_op jit(solution)/shard_map/pallas_call | solution.py:594

commit v5 on v4

--- a/solution.py
+++ b/solution.py
@@ -461,8 +461,8 @@
     cross(0, 0)
     landed(0, 0)
     xsend_w(1, 1)
+    plane_x(1, 0)
     plane_own(1, 0)
-    plane_x(1, 0)
     gates(0)
     cross(0, 1)
     landed(0, 1)
@@ -470,8 +470,8 @@
     landed_d(0)
     compute(0)
     rs_first(0)
+    xsend_d(1)
     plane_x(1, 1)
-    xsend_d(1)
     rs_far(0, 0)
     if C > 1:
         rs_far(0, 1)

time: 135 us -> 136 us (level)
  no operation moved by 1% of the time
where the time goes in v5:
time: 136 us
  Pallas kernels  135 us (99%)
    pallas_call x1, Pallas kernels, per_device(): pl.pallas_call(functools.partial(kernel, G, n, T), out_shape=(pltpu.VMEM(...  130 us
    pallas_call x1, Pallas kernels, per_device(): pl.pallas_call(write_out, out_shape=(jax.ShapeDtypeStruct((L, n, R, FFb),...  4.99 us

profile of v5, /device:TPU:0, one launch (start us, length us, event | category | flops | bytes accessed | tf_op | source)
XLA Modules:
  0.0 135.8 jit_solution(6175141809208035531)
XLA Ops:
  0.6 130.1 %shard_map.84 = (bf16[2,2,8,256,512]{4,3,2,1,0:T(8,128)(2,1)S(1)}, bf16[2,4,512,512]{3,2,1,0:T(8,128)(2,1)S(1)}, bf16[2,8,32,2048]{3,2,1,0:T(8,128)(2,1)S(1)}) custom-call(bf16[8,32,2048]{2,1,0:T(8,128)(2,1)} %bitcast.4, f32[2,256]{1,0:T(2,128)} %gain_h.1, f32[2,256,1024]{2,1,0:T(8,128)} %gate_h.1, f32[2,256,1024]{2,1,0:T(8,128)} %up_h.1, f32[2,512,512]{2,1,0:T(8,128)} %down_h.1), custom_call_target="tpu_custom_call" | custom-call | tf_op jit(solution)/shard_map/pallas_call | solution.py:562
  130.8 5.0 %shard_map.85 = (bf16[2,8,256,512]{3,2,1,0:T(8,128)(2,1)}, bf16[2,8,256,512]{3,2,1,0:T(8,128)(2,1)}, bf16[2,512,2048]{2,1,0:T(8,128)(2,1)}, bf16[8,32,2048]{2,1,0:T(8,128)(2,1)}) custom-call(bf16[2,2,8,256,512]{4,3,2,1,0:T(8,128)(2,1)S(1)} %get-tuple-element.11.wall, bf16[2,4,512,512]{3,2,1,0:T(8,128)(2,1)S(1)} %get-tuple-element.12.dn, ...), custom_call_target="tpu_custom_call" | custom-call | tf_op jit(solution)/shard_map/pallas_call | solution.py:594

commit v6 on v5

--- a/solution.py
+++ b/solution.py
@@ -470,8 +470,8 @@
     landed_d(0)
     compute(0)
     rs_first(0)
+    plane_x(1, 1)
     xsend_d(1)
-    plane_x(1, 1)
     rs_far(0, 0)
     if C > 1:
         rs_far(0, 1)

time: 136 us -> 135 us (level)
  no operation moved by 1% of the time
where the time goes in v6:
time: 135 us
  Pallas kernels  134 us (99%)
    pallas_call x1, Pallas kernels, per_device(): pl.pallas_call(functools.partial(kernel, G, n, T), out_shape=(pltpu.VMEM(...  129 us
    pallas_call x1, Pallas kernels, per_device(): pl.pallas_call(write_out, out_shape=(jax.ShapeDtypeStruct((L, n, R, FFb),...  4.99 us

profile of v6, /device:TPU:0, one launch (start us, length us, event | category | flops | bytes accessed | tf_op | source)
XLA Modules:
  0.0 134.8 jit_solution(4552673386107781590)
XLA Ops:
  0.6 129.2 %shard_map.84 = (bf16[2,2,8,256,512]{4,3,2,1,0:T(8,128)(2,1)S(1)}, bf16[2,4,512,512]{3,2,1,0:T(8,128)(2,1)S(1)}, bf16[2,8,32,2048]{3,2,1,0:T(8,128)(2,1)S(1)}) custom-call(bf16[8,32,2048]{2,1,0:T(8,128)(2,1)} %bitcast.4, f32[2,256]{1,0:T(2,128)} %gain_h.1, f32[2,256,1024]{2,1,0:T(8,128)} %gate_h.1, f32[2,256,1024]{2,1,0:T(8,128)} %up_h.1, f32[2,512,512]{2,1,0:T(8,128)} %down_h.1), custom_call_target="tpu_custom_call" | custom-call | tf_op jit(solution)/shard_map/pallas_call | solution.py:562
  129.9 5.0 %shard_map.85 = (bf16[2,8,256,512]{3,2,1,0:T(8,128)(2,1)}, bf16[2,8,256,512]{3,2,1,0:T(8,128)(2,1)}, bf16[2,512,2048]{2,1,0:T(8,128)(2,1)}, bf16[8,32,2048]{2,1,0:T(8,128)(2,1)}) custom-call(bf16[2,2,8,256,512]{4,3,2,1,0:T(8,128)(2,1)S(1)} %get-tuple-element.11.wall, bf16[2,4,512,512]{3,2,1,0:T(8,128)(2,1)S(1)} %get-tuple-element.12.dn, ...), custom_call_target="tpu_custom_call" | custom-call | tf_op jit(solution)/shard_map/pallas_call | solution.py:594
